TPU v7x, 32 devices: a whole 2x2x4 slice. The times are simulated.
32 devices in a mesh: gr: 2 (over x), fs: 8 (over z, y), tp: 2 (over core).
Axes of the slice: x: 2, y: 2, z: 4, core: 2. Of those that a mesh axis runs over, the one named last changes fastest.
Arguments:
- tokens: bfloat16 [2816, 2048], P(('gr', 'fs')), may hold values from -6 to 6
- expert_ids: int32 [2816, 8], P(('gr', 'fs')), may hold values from 0 to 15, all different within a row; in each aligned block of 176 rows (0 to 175, 176 to 351, ...) at most 110 rows name the same one
- route_weight: float32 [2816, 8], P(('gr', 'fs')), may hold values from 0.05 to 1
- norm_gain: float32 [2048], P('tp'), may hold values from 0.1 to 1.9
- expert_gate: float32 [16, 512, 2048], P('gr', 'fs', 'tp'), may hold values from -0.125 to 0.125
- expert_up: float32 [16, 512, 2048], P('gr', 'fs', 'tp'), may hold values from -0.125 to 0.125
- expert_down: float32 [16, 512, 2048], P('gr', 'fs', 'tp'), may hold values from -0.25 to 0.25
- shared_gate: float32 [512, 2048], P('fs', 'tp'), may hold values from -0.125 to 0.125
- shared_up: float32 [512, 2048], P('fs', 'tp'), may hold values from -0.125 to 0.125
- shared_down: float32 [512, 2048], P('fs', 'tp'), may hold values from -0.25 to 0.25
Outputs:
- mixed: bfloat16 [2816, 2048], P(('gr', 'fs'), 'tp')
- new_gate: bfloat16 [2, 8, 512, 2048], P(None, 'fs', None, 'tp')
- new_up: bfloat16 [2, 8, 512, 2048], P(None, 'fs', None, 'tp')
- new_down: bfloat16 [2, 8, 512, 2048], P(None, 'fs', None, 'tp')
- new_shared_gate: bfloat16 [512, 2048], P(None, 'tp')
- new_shared_up: bfloat16 [512, 2048], P(None, 'tp')
- new_shared_down: bfloat16 [512, 2048], P(None, 'tp')
Inputs may be any that keep to these rules, and one draw needn't show every extreme that they name: `expert_ids`: each row names 8 different experts; within each aligned block of 176 rows no expert is named by more than 110 rows, a bound that some block reaches.
All inputs are finite; a program needn't handle non-finite values.
Results may differ from a plain program's by a relative error of at most 0.022.
Values may be sent and summed in bfloat16 or wider, within the bound.
A program may use at most 128 MiB of HBM per device.

v0:
```python
import functools

import jax
import jax.numpy as jnp
from jax import lax
from jax.experimental import pallas as pl
from jax.experimental.pallas import tpu as pltpu
from jax.sharding import PartitionSpec as P

route_scale = 2.5
norm_eps = 1e-06
vmem_bytes = 67043328


def fold_gain(weight, gain):
    return (weight * gain).astype(jnp.bfloat16)


def silu(v):
    return v / (1.0 + jnp.exp(-v))


def handover(
    dims,
    tok,
    w0,
    w1,
    w2,
    s0,
    s1,
    s2,
    mixed,
    o0,
    o1,
    o2,
    q0,
    q1,
    q2,
    n0,
    n1,
    n2,
    h0,
    h1,
    h2,
    xs,
    pout,
    pin,
    act,
    oz,
    rety,
    ret,
    psh,
    pshin,
    local_sem,
    out_sem,
    tok_send,
    tok_recv,
    w_send,
    w_recv,
    x_send,
    x_recv,
    sh_send,
    sh_recv,
    shx_send,
    shx_recv,
    p_send,
    p_recv,
    a_send,
    a_recv,
    ry_send,
    ry_recv,
    r_send,
    r_recv,
    ps_send,
    ps_recv,
):
    G, S, TP, T, C, H, F, SF, slots, Y = dims
    Z = S // Y
    E = G * S
    SH = SF * S
    NB = S // TP
    NH = NB * T
    gi, si, ti = lax.axis_index("gr"), lax.axis_index("fs"), lax.axis_index("tp")
    zi, yi = si // Y, lax.rem(si, Y)
    w, new, sh, shn = (w0, w1, w2), (n0, n1, n2), (s0, s1, s2), (h0, h1, h2)
    outs, shouts = (o0, o1, o2), (q0, q1, q2)

    def rdma(src, dst, ssem, rsem, dev):
        return pltpu.make_async_remote_copy(
            src_ref=src,
            dst_ref=dst,
            send_sem=ssem,
            recv_sem=rsem,
            device_id=dev,
            device_id_type=pl.DeviceIdType.MESH,
        )

    def rows(start, step, size):
        return pl.ds(pl.multiple_of(start * step, step), size)

    def each(lo, hi, fn):
        def step(i, c):
            fn(i)
            return c

        lax.fori_loop(lo, hi, step, 0)

    def fs_peer(k):
        return lax.rem(si + k, S)

    def fs_from(k):
        return lax.rem(si + S - k, S)

    def gr_peer(k):
        return lax.rem(gi + k, G)

    def tp_peer(k):
        return lax.rem(ti + k, TP)

    barrier = pltpu.get_barrier_semaphore()

    def greet(axis, peer, n):
        each(
            1,
            n,
            lambda k: pl.semaphore_signal(
                barrier,
                inc=1,
                device_id={axis: peer(k)},
                device_id_type=pl.DeviceIdType.MESH,
            ),
        )

    greet("fs", fs_peer, S)
    greet("gr", gr_peer, G)
    greet("tp", tp_peer, TP)
    pl.semaphore_wait(barrier, S + G + TP - 3)

    def w_copy(m, d, s):
        return rdma(
            w[m].at[d], new[m].at[gi, rows(s, F, F)], w_send.at[m, d], w_recv.at[m, s], {"fs": d}
        )

    def spread(block, s, up, down, act_on, own=False):
        src, place, ssem, rsem, after = block
        at = place(s)

        def hop(way, dev):
            act_on(rdma(src if own else at, at, ssem.at[s, way], rsem.at[s], {"fs": dev}))

        if up:
            pl.when(zi < Z - 1)(lambda: hop(0, si + Y))
        if down:
            pl.when(zi > 0)(lambda: hop(1, si - Y))

        def across(k):
            y = lax.rem(yi + k, Y)
            hop(2 + y, zi * Y + y)

        each(1, Y, across)

    def shx_copy(m, s, g, dev):
        at = sh_place(m, s, g)
        return rdma(at, at, shx_send.at[m, s, dev], shx_recv.at[m, s, g], {"gr": dev})

    def arrive(block, s):
        src, place, ssem, rsem, after = block
        rdma(place(s), place(s), ssem.at[s, 0], rsem.at[s], {"fs": fs_peer(1)}).wait_recv()
        if after is not None:
            after(s)

    def start(c):
        c.start()

    def sent(c):
        c.wait_send()

    def relay(block, step, act_on=start):
        def from_below():
            s = si - step * Y
            if act_on is start:
                arrive(block, s)
            spread(block, s, True, False, act_on)

        def from_above():
            s = si + step * Y
            if act_on is start:
                arrive(block, s)
            spread(block, s, False, True, act_on)

        pl.when(zi >= step)(from_below)
        pl.when(zi + step < Z)(from_above)

    def others_arrive(block, step):
        def at(z):
            each(1, Y, lambda k: arrive(block, z * Y + lax.rem(yi + k, Y)))

        if step == 0:
            at(zi)
        else:
            pl.when(zi >= step)(lambda: at(zi - step))
            pl.when(zi + step < Z)(lambda: at(zi + step))

    def block_sent(block):
        spread(block, si, True, True, sent, own=True)
        for step in range(1, Z):
            relay(block, step, sent)

    def sh_place(m, s, g):
        return shn[m].at[rows(s, SF, SF), rows(g, C // G, C // G)]

    def sh_block(m):
        return (
            sh[m].at[:, rows(gi, C // G, C // G)],
            lambda s: sh_place(m, s, gi),
            sh_send.at[m],
            sh_recv.at[m],
            lambda s: each(1, G, lambda j: shx_copy(m, s, gi, gr_peer(j)).start()),
        )

    tok_block = (tok, lambda s: xs.at[rows(s, T, T)], tok_send, tok_recv, None)
    sh_blocks = [sh_block(m) for m in range(3)]

    def shared_step(step):
        for block in sh_blocks:
            if step < Z:
                relay(block, step)
            others_arrive(block, step - 1)

    def x_copy(m, s, g, dev, own=False):
        place = new[m].at[g, rows(s, F, F)]
        src = w[m].at[s] if own else place
        return rdma(src, place, x_send.at[m, s, dev], x_recv.at[m, s, g], {"gr": dev})

    def local_copies():
        return (
            [pltpu.make_async_copy(w[m].at[si], new[m].at[gi, rows(si, F, F)], local_sem.at[m]) for m in range(3)]
            + [pltpu.make_async_copy(sh[m], shn[m].at[rows(si, SF, SF)], local_sem.at[3 + m]) for m in range(3)]
            + [pltpu.make_async_copy(tok, xs.at[rows(si, T, T)], local_sem.at[6])]
        )

    def send_weight(m):
        each(1, S, lambda k: w_copy(m, fs_peer(k), si).start())

    for m in range(3):
        each(1, G, lambda j, m=m: x_copy(m, si, gi, gr_peer(j), own=True).start())
    spread(tok_block, si, True, True, start, own=True)
    send_weight(0)
    for copy in local_copies():
        copy.start()

    def forward(m, lo=1, hi=S):
        def one(k):
            s = fs_from(k)
            w_copy(m, s, s).wait_recv()
            each(1, G, lambda j: x_copy(m, s, gi, gr_peer(j)).start())

        each(lo, hi, one)

    def x_arrive(m, g):
        each(0, S, lambda s: x_copy(m, s, g, g).wait_recv())

    def p_copy(j, t, s):
        return rdma(
            pout.at[j if slots > 1 else 0, t], pin.at[j, s], p_send.at[j, t], p_recv.at[j, s], {"tp": t}
        )

    def a_copy(j, t, s):
        place = act.at[j, rows(s, NH, NH)]
        return rdma(place, place, a_send.at[j, t], a_recv.at[j, s], {"tp": t})

    def first_matmuls(j):
        g = gr_peer(j)
        slot = j if slots > 1 else 0
        for q in range(TP):
            t = tp_peer(1 + q)

            def block(b, t=t):
                x = xs[rows(t * NB + b, T, T), 0:C]
                for m in range(2):
                    part = lax.dot_general(
                        x, new[m][g], (((1,), (1,)), ((), ())), preferred_element_type=jnp.float32
                    )
                    pout[slot, t, rows(b, T, T), m * H : (m + 1) * H] = part.astype(jnp.bfloat16)

            each(0, NB, block)
            if q < TP - 1:
                p_copy(j, t, ti).start()

    def activations(j):
        g = gr_peer(j)
        slot = j if slots > 1 else 0
        expert = g * S + si
        for q in range(1, TP):
            t = tp_peer(q)
            p_copy(j, t, t).wait_recv()

        def block(b):
            r = rows(b, T, T)
            pre = pout[slot, ti, r, :].astype(jnp.float32)
            for q in range(1, TP):
                pre = pre + pin[j, tp_peer(q), r, :].astype(jnp.float32)
            at = rows(ti * NB + b, T, T)
            coded = xs[at, C:].astype(jnp.float32)
            lane = lax.broadcasted_iota(jnp.int32, coded.shape, 1)
            share = jnp.sum(
                jnp.where((lane == expert) | (lane == expert + E), coded, 0.0), axis=1, keepdims=True
            )
            value = silu(pre[:, :H]) * pre[:, H:] * share
            act[j, at, :] = value.astype(jnp.bfloat16)

        each(0, NB, block)
        for q in range(1, TP):
            a_copy(j, tp_peer(q), ti).start()

    if Z > 1:
        relay(tok_block, 1)
    send_weight(1)
    forward(0)
    for step in range(2, Z):
        relay(tok_block, step)
    send_weight(2)
    for block in sh_blocks:
        spread(block, si, True, True, start, own=True)
    forward(1)
    for copy in local_copies():
        copy.wait()
    for step in range(Z):
        others_arrive(tok_block, step)
    for j in range(G):
        if j > 0:
            for m in range(2):
                x_arrive(m, gr_peer(j))
            if slots == 1:
                for q in range(1, TP):
                    p_copy(j - 1, tp_peer(q), ti).wait_send()
        first_matmuls(j)
        if j == 1:
            forward(2, S // 2, S)
        activations(j)
        if j == 0:
            forward(2, 1, S // 2 if G > 1 else S)
    shared_step(1)

    for m in range(2):
        pltpu.make_async_copy(new[m], outs[m], out_sem.at[m]).start()
    for j in range(1, G):
        x_arrive(2, gr_peer(j))
    pltpu.make_async_copy(new[2], outs[2], out_sem.at[2]).start()

    def ry_copy(z, y, src):
        return rdma(
            oz.at[rows(z * Y + y, T, T)],
            rety.at[z, src],
            ry_send.at[z, y],
            ry_recv.at[z, src],
            {"fs": zi * Y + y},
        )

    def r_copy(z, up, dist):
        slot = Z if dist == 1 and not up else z
        return rdma(
            oz.at[rows(z * Y + yi, T, T)],
            ret.at[slot],
            r_send.at[z],
            r_recv.at[slot],
            {"fs": si + Y if up else si - Y},
        )

    def far_first(fn):
        for dist in range(Z - 1, -1, -1):
            pl.when(zi + dist < Z)(functools.partial(fn, zi + dist, True, dist))
            if dist:
                pl.when(zi >= dist)(functools.partial(fn, zi - dist, False, dist))

    for q in range(1, TP):
        for j in range(G):
            a_copy(j, tp_peer(q), tp_peer(q)).wait_recv()

    def down_block(z, up, dist):
        def column(k):
            y = lax.rem(yi + k, Y)
            at = rows(z * Y + y, T, T)
            total = jnp.zeros((T, C), jnp.float32)
            for j in range(G):
                total = total + jnp.dot(
                    act[j, at, :], new[2][gr_peer(j)], preferred_element_type=jnp.float32
                )
            oz[at, :] = total.astype(jnp.bfloat16)
            pl.when(y != yi)(lambda: ry_copy(z, y, yi).start())

        each(1, Y + 1, column)

    far_first(down_block)
    if Z > 1:
        shared_step(2)

    def add_far(z, slot):
        at = rows(z * Y + yi, T, T)
        rdma(
            ret.at[slot], ret.at[slot], r_send.at[z], r_recv.at[slot], {"fs": fs_peer(1)}
        ).wait_recv()
        total = oz[at, :].astype(jnp.float32) + ret[slot].astype(jnp.float32)
        oz[at, :] = total.astype(jnp.bfloat16)

    def column_sum(z, up, dist):
        at = rows(z * Y + yi, T, T)
        total = oz[at, :].astype(jnp.float32)
        for k in range(1, Y):
            y = lax.rem(yi + k, Y)
            ry_copy(z, y, y).wait_recv()
            total = total + rety[z, y].astype(jnp.float32)
        oz[at, :] = total.astype(jnp.bfloat16)
        if dist == 0 or up:
            pl.when(zi > 0)(lambda: add_far(z, z))
        if dist == 0:
            pl.when(zi < Z - 1)(lambda: add_far(z, Z))
        elif not up:
            pl.when(zi < Z - 1)(lambda: add_far(z, z))
        if dist:
            r_copy(z, up, dist).start()

    far_first(column_sum)
    for step in range(3, Z + 1):
        shared_step(step)

    def shared_arrive(m):
        each(
            1,
            S,
            lambda k: each(
                1, G, lambda j: shx_copy(m, fs_from(k), gr_peer(j), gr_peer(j)).wait_recv()
            ),
        )

    def ps_copy(t, s):
        return rdma(psh, pshin.at[s], ps_send.at[t], ps_recv.at[s], {"tp": t})

    for m in range(2):
        shared_arrive(m)
        part = lax.dot_general(
            xs[rows(si, T, T), 0:C],
            shn[m][...],
            (((1,), (1,)), ((), ())),
            preferred_element_type=jnp.float32,
        )
        psh[:, m * SH : (m + 1) * SH] = part.astype(jnp.bfloat16)
        pltpu.make_async_copy(shn[m], shouts[m], out_sem.at[3 + m]).start()
    for q in range(1, TP):
        ps_copy(tp_peer(q), ti).start()
    shared_arrive(2)
    pltpu.make_async_copy(shn[2], shouts[2], out_sem.at[5]).start()
    pre = psh[...].astype(jnp.float32)
    for q in range(1, TP):
        t = tp_peer(q)
        ps_copy(t, t).wait_recv()
        pre = pre + pshin[t].astype(jnp.float32)
    shared_act = (silu(pre[:, :SH]) * pre[:, SH:]).astype(jnp.bfloat16)
    total = jnp.dot(shared_act, shn[2][...], preferred_element_type=jnp.float32)
    total = total + oz[rows(si, T, T), :].astype(jnp.float32)
    mixed[...] = total.astype(jnp.bfloat16)

    for m in range(3):
        pltpu.make_async_copy(new[m], outs[m], out_sem.at[m]).wait()
        pltpu.make_async_copy(shn[m], shouts[m], out_sem.at[3 + m]).wait()
        each(1, S, lambda k, m=m: w_copy(m, fs_peer(k), si).wait_send())
        block_sent(sh_blocks[m])
        each(
            1,
            S,
            lambda k, m=m: each(
                1, G, lambda j: shx_copy(m, fs_from(k), gi, gr_peer(j)).wait_send()
            ),
        )
        each(0, S, lambda s, m=m: each(1, G, lambda j: x_copy(m, s, gi, gr_peer(j)).wait_send()))
    block_sent(tok_block)
    each(0, Z, lambda z: each(1, Y, lambda k: ry_copy(z, lax.rem(yi + k, Y), yi).wait_send()))

    def r_sent(z, up, dist):
        if dist:
            r_copy(z, up, dist).wait_send()

    far_first(r_sent)
    for q in range(1, TP):
        t = tp_peer(q)
        ps_copy(t, ti).wait_send()
        for j in range(G):
            if slots > 1 or j == G - 1:
                p_copy(j, t, ti).wait_send()
            a_copy(j, t, ti).wait_send()


def body(
    Y,
    tokens,
    expert_ids,
    route_weight,
    norm_gain,
    expert_gate,
    expert_up,
    expert_down,
    shared_gate,
    shared_up,
    shared_down,
):
    G, S, TP = lax.axis_size("gr"), lax.axis_size("fs"), lax.axis_size("tp")
    T, C = tokens.shape[0], expert_gate.shape[2]
    F, SF = expert_gate.shape[1], shared_gate.shape[0]
    H, SH = F * S, SF * S
    E, N = G * S, S * T
    NH = N // TP
    lanes = -(-2 * E // 128) * 128
    bf16 = jnp.bfloat16

    tok_float = tokens.astype(jnp.float32)
    normed = (
        tok_float * lax.rsqrt(jnp.mean(tok_float * tok_float, axis=1, keepdims=True) + norm_eps)
    ).astype(bf16)
    normed_cols = lax.dynamic_slice_in_dim(normed, lax.axis_index("tp") * C, C, 1)
    share = route_weight / jnp.sum(route_weight, axis=1, keepdims=True) * route_scale
    lane = jnp.arange(lanes, dtype=jnp.int32)[None, None, :]
    dense = jnp.sum(
        jnp.where(expert_ids[:, :, None] == lane % E, share[:, :, None], 0.0), axis=1
    )
    high = dense.astype(bf16)
    low = (dense - lax.reduce_precision(dense, 8, 7)).astype(bf16)
    place = lane[0]
    coded = jnp.where(place < E, high, jnp.where(place < 2 * E, low, 0))
    payload = jnp.concatenate([normed_cols, coded.astype(bf16)], axis=1)

    weights = (
        fold_gain(expert_gate, norm_gain),
        fold_gain(expert_up, norm_gain),
        expert_down.astype(bf16),
    )
    shared = (
        fold_gain(shared_gate, norm_gain),
        fold_gain(shared_up, norm_gain),
        shared_down.astype(bf16),
    )
    row_bytes = 2 * (2 * G * 2 * H + G * H + 3 * C + lanes)
    slots = G if N * row_bytes < vmem_bytes * 3 // 5 else 1
    dims = (G, S, TP, T, C, H, F, SF, slots, Y)
    vmem, hbm = pl.BlockSpec(memory_space=pltpu.VMEM), pl.BlockSpec(memory_space=pl.ANY)
    dma = pltpu.SemaphoreType.DMA
    results = pl.pallas_call(
        functools.partial(handover, dims),
        out_shape=[jax.ShapeDtypeStruct((T, C), bf16)]
        + [jax.ShapeDtypeStruct((G, H, C), bf16)] * 3
        + [jax.ShapeDtypeStruct((SH, C), bf16)] * 3,
        in_specs=[vmem] * 7,
        out_specs=[vmem] + [hbm] * 6,
        scratch_shapes=[pltpu.VMEM((G, H, C), bf16)] * 3
        + [pltpu.VMEM((SH, C), bf16)] * 3
        + [
            pltpu.VMEM((N, C + lanes), bf16),
            pltpu.VMEM((slots, TP, NH, 2 * H), bf16),
            pltpu.VMEM((G, TP, NH, 2 * H), bf16),
            pltpu.VMEM((G, N, H), bf16),
            pltpu.VMEM((N, C), bf16),
            pltpu.VMEM((S // Y, Y, T, C), bf16),
            pltpu.VMEM((S // Y + 1, T, C), bf16),
            pltpu.VMEM((T, 2 * SH), bf16),
            pltpu.VMEM((TP, T, 2 * SH), bf16),
            dma((7,)),
            dma((6,)),
            dma((S, 2 + Y)),
            dma((S,)),
            dma((3, S)),
            dma((3, S)),
            dma((3, S, G)),
            dma((3, S, G)),
            dma((3, S, 2 + Y)),
            dma((3, S)),
            dma((3, S, G)),
            dma((3, S, G)),
            dma((G, TP)),
            dma((G, TP)),
            dma((G, TP)),
            dma((G, TP)),
            dma((S // Y, Y)),
            dma((S // Y, Y)),
            dma((S // Y,)),
            dma((S // Y + 1,)),
            dma((TP,)),
            dma((TP,)),
        ],
        compiler_params=pltpu.CompilerParams(
            collective_id=0, has_side_effects=True, vmem_limit_bytes=vmem_bytes
        ),
        name="handover",
    )(payload, *weights, *shared)
    mixed = results[0]
    whole = [r.reshape(G, 1, H, C) for r in results[1:4]]
    return (mixed, *whole, *results[4:])


def line_length(mesh):
    places = [d.coords for d in mesh.devices[0, :, 0]]
    axis = [i for i in range(3) if places[0][i] != places[1][i]][0]
    count = 0
    for place in places:
        if any(place[i] != places[0][i] for i in range(3) if i != axis):
            break
        count += 1
    return count if len(places) % count == 0 else len(places)


def solution(mesh):
    placed = (
        P(("gr", "fs"), None),
        P(("gr", "fs"), None),
        P(("gr", "fs"), None),
        P("tp"),
        P("gr", "fs", "tp"),
        P("gr", "fs", "tp"),
        P("gr", "fs", "tp"),
        P("fs", "tp"),
        P("fs", "tp"),
        P("fs", "tp"),
    )
    return jax.shard_map(
        functools.partial(body, line_length(mesh)),
        mesh=mesh,
        in_specs=placed,
        out_specs=(
            P(("gr", "fs"), "tp"),
            P(None, "fs", None, "tp"),
            P(None, "fs", None, "tp"),
            P(None, "fs", None, "tp"),
            P(None, "tp"),
            P(None, "tp"),
            P(None, "tp"),
        ),
        check_vma=False,
    )
```

profile of v0, /device:TPU:1, one launch (start us, length us, event | category | flops | bytes accessed | tf_op | source)
XLA Modules:
  0.0 206.1 jit_solution(10394341972154389177)
XLA Ops:
  0.7 1.5 multiply_reduce_fusion
  2.1 0.7 reduce_sum.28
  2.9 0.7 divide_multiply_fusion
  3.7 0.8 copy.22
  4.5 0.4 select_reduce_fusion
  5.0 1.7 convert_element_type.41.s2
  6.7 1.8 multiply_convert_fusion.2
  8.5 1.1 convert_element_type.38.w2
  9.6 0.1 convert_element_type.32
  9.8 0.1 fusion
  9.9 0.8 pad_maximum_fusion.tok
  10.7 0.8 copy-done.4
  11.5 1.9 multiply_convert_fusion
  13.5 179.8 %handover.1 = (bf16[176,1024]{1,0:T(8,128)(2,1)}, bf16[2,512,1024]{2,1,0:T(8,128)(2,1)}, bf16[2,512,1024]{2,1,0:T(8,128)(2,1)}, bf16[2,512,1024]{2,1,0:T(8,128)(...) custom-call(bf16[176,1152]{1,0:T(8,128)(2,1)} %pad_maximum_fusion.tok, ...), custom_call_target="tpu_custom_call" | custom-call | tf_op jit(solution)/shard_map/handover/pallas_call | solution.py:546
  193.3 1.7 copy.34
  195.0 3.2 %copy.35 = bf16[2,1,512,1024]{3,2,1,0:T(8,128)(2,1)} copy(bf16[2,1,512,1024]{3,2,1,0:T(8,128)(2,1)} %bitcast.11) | data formatting | bytes 4194304
  198.3 1.3 copy.36
  199.6 1.0 copy-done.2
  200.6 1.3 copy.37
  201.9 0.6 copy-done.8
  202.6 1.0 copy.38
  203.5 0.6 copy-done.7
  204.2 1.0 copy.39
  205.1 1.0 copy.40
  (21 shorter events, 0.2 us)
Async XLA Ops:
  0.6 7.9 %copy-start.1 = (f32[8,64,1024]{2,1,0:T(8,128)S(1)}, f32[8,64,1024]{2,1,0:T(8,128)}, u32[]{:S(2)}) copy-start(f32[8,64,1024]{2,1,0:T(8,128)} %param.16) | copy-start | bytes 6291460
  5.0 4.6 %copy-start = (bf16[176,2048]{1,0:T(8,128)(2,1)S(1)}, bf16[176,2048]{1,0:T(8,128)(2,1)}, u32[]{:S(2)}) copy-start(bf16[176,2048]{1,0:T(8,128)(2,1)} %param.10) | copy-start | bytes 2162692
  8.5 2.2 %copy-start.5 = (f32[8,64,1024]{2,1,0:T(8,128)S(1)}, f32[8,64,1024]{2,1,0:T(8,128)}, u32[]{:S(2)}) copy-start(f32[8,64,1024]{2,1,0:T(8,128)} %param.14) | copy-start | bytes 6291460
  9.6 1.9 copy-start.4
  9.6 1.9 copy-start.9
  195.0 3.2 %copy-start.3 = (bf16[2,512,1024]{2,1,0:T(8,128)(2,1)S(1)}, bf16[2,512,1024]{2,1,0:T(8,128)(2,1)}, u32[]{:S(2)}) copy-start(bf16[2,512,1024]{2,1,0:T(8,128)(2,1)} %get-tuple-element.16) | copy-start | bytes 6291460
  198.2 2.3 %copy-start.2 = (bf16[2,512,1024]{2,1,0:T(8,128)(2,1)S(1)}, bf16[2,512,1024]{2,1,0:T(8,128)(2,1)}, u32[]{:S(2)}) copy-start(bf16[2,512,1024]{2,1,0:T(8,128)(2,1)} %get-tuple-element.17) | copy-start | bytes 6291460
  200.6 2.0 copy-start.8
  202.6 1.6 copy-start.7
  202.6 2.6 %copy-start.6 = (bf16[512,1024]{1,0:T(8,128)(2,1)S(1)}, bf16[512,1024]{1,0:T(8,128)(2,1)}, u32[]{:S(2)}) copy-start(bf16[512,1024]{1,0:T(8,128)(2,1)} %get-tuple-element.54) | copy-start | bytes 3145732
where the time goes:
time: 207 us; the launch traced here: 206 us
  Pallas kernels  180 us (87%)
  local copies, waits for them, and re-layouts  14.6 us (7%)
  other arithmetic  11 us (5%)
    pallas_call x1, Pallas kernels, body(): pl.pallas_call(functools.partial(handover, dims), out_shape=[jax.ShapeDty...  180 us
    unnamed x28, local copies, waits for them, and re-layouts  14.5 us

commit v1 on v0

--- a/solution.py
+++ b/solution.py
@@ -30,12 +30,6 @@
     s1,
     s2,
     mixed,
-    o0,
-    o1,
-    o2,
-    q0,
-    q1,
-    q2,
     n0,
     n1,
     n2,
@@ -52,7 +46,6 @@
     psh,
     pshin,
     local_sem,
-    out_sem,
     tok_send,
     tok_recv,
     w_send,
@@ -83,7 +76,6 @@
     gi, si, ti = lax.axis_index("gr"), lax.axis_index("fs"), lax.axis_index("tp")
     zi, yi = si // Y, lax.rem(si, Y)
     w, new, sh, shn = (w0, w1, w2), (n0, n1, n2), (s0, s1, s2), (h0, h1, h2)
-    outs, shouts = (o0, o1, o2), (q0, q1, q2)
 
     def rdma(src, dst, ssem, rsem, dev):
         return pltpu.make_async_remote_copy(
@@ -342,11 +334,8 @@
             forward(2, 1, S // 2 if G > 1 else S)
     shared_step(1)
 
-    for m in range(2):
-        pltpu.make_async_copy(new[m], outs[m], out_sem.at[m]).start()
     for j in range(1, G):
         x_arrive(2, gr_peer(j))
-    pltpu.make_async_copy(new[2], outs[2], out_sem.at[2]).start()
 
     def ry_copy(z, y, src):
         return rdma(
@@ -445,11 +434,9 @@
             preferred_element_type=jnp.float32,
         )
         psh[:, m * SH : (m + 1) * SH] = part.astype(jnp.bfloat16)
-        pltpu.make_async_copy(shn[m], shouts[m], out_sem.at[3 + m]).start()
     for q in range(1, TP):
         ps_copy(tp_peer(q), ti).start()
     shared_arrive(2)
-    pltpu.make_async_copy(shn[2], shouts[2], out_sem.at[5]).start()
     pre = psh[...].astype(jnp.float32)
     for q in range(1, TP):
         t = tp_peer(q)
@@ -461,8 +448,6 @@
     mixed[...] = total.astype(jnp.bfloat16)
 
     for m in range(3):
-        pltpu.make_async_copy(new[m], outs[m], out_sem.at[m]).wait()
-        pltpu.make_async_copy(shn[m], shouts[m], out_sem.at[3 + m]).wait()
         each(1, S, lambda k, m=m: w_copy(m, fs_peer(k), si).wait_send())
         block_sent(sh_blocks[m])
         each(
@@ -488,6 +473,36 @@
             if slots > 1 or j == G - 1:
                 p_copy(j, t, ti).wait_send()
             a_copy(j, t, ti).wait_send()
+
+
+def emit_kernel(*refs):
+    n = len(refs) // 2
+    sem = refs[-1]
+    copies = []
+    for i in range(n):
+        dst = refs[n + i]
+        if len(dst.shape) == 4:
+            dst = dst.at[:, 0]
+        copies.append(pltpu.make_async_copy(refs[i], dst, sem.at[i]))
+    for c in copies:
+        c.start()
+    for c in copies:
+        c.wait()
+
+
+def emit(results, G):
+    bf16 = jnp.bfloat16
+    shapes = [r.shape if len(r.shape) < 3 else (r.shape[0], 1) + r.shape[1:] for r in results]
+    n = len(results)
+    return pl.pallas_call(
+        emit_kernel,
+        out_shape=[jax.ShapeDtypeStruct(s, bf16) for s in shapes],
+        in_specs=[pl.BlockSpec(memory_space=pltpu.VMEM)] * n,
+        out_specs=[pl.BlockSpec(memory_space=pl.ANY)] * n,
+        scratch_shapes=[pltpu.SemaphoreType.DMA((n,))],
+        compiler_params=pltpu.CompilerParams(vmem_limit_bytes=vmem_bytes // 2),
+        name="emit",
+    )(*results)
 
 
 def body(
@@ -543,16 +558,15 @@
     dims = (G, S, TP, T, C, H, F, SF, slots, Y)
     vmem, hbm = pl.BlockSpec(memory_space=pltpu.VMEM), pl.BlockSpec(memory_space=pl.ANY)
     dma = pltpu.SemaphoreType.DMA
+    out_bytes = 2 * C * (T + 3 * G * H + 3 * SH)
     results = pl.pallas_call(
         functools.partial(handover, dims),
-        out_shape=[jax.ShapeDtypeStruct((T, C), bf16)]
-        + [jax.ShapeDtypeStruct((G, H, C), bf16)] * 3
-        + [jax.ShapeDtypeStruct((SH, C), bf16)] * 3,
+        out_shape=[pltpu.VMEM((T, C), bf16)]
+        + [pltpu.VMEM((G, H, C), bf16)] * 3
+        + [pltpu.VMEM((SH, C), bf16)] * 3,
         in_specs=[vmem] * 7,
-        out_specs=[vmem] + [hbm] * 6,
-        scratch_shapes=[pltpu.VMEM((G, H, C), bf16)] * 3
-        + [pltpu.VMEM((SH, C), bf16)] * 3
-        + [
+        out_specs=[vmem] * 7,
+        scratch_shapes=[
             pltpu.VMEM((N, C + lanes), bf16),
             pltpu.VMEM((slots, TP, NH, 2 * H), bf16),
             pltpu.VMEM((G, TP, NH, 2 * H), bf16),
@@ -563,7 +577,6 @@
             pltpu.VMEM((T, 2 * SH), bf16),
             pltpu.VMEM((TP, T, 2 * SH), bf16),
             dma((7,)),
-            dma((6,)),
             dma((S, 2 + Y)),
             dma((S,)),
             dma((3, S)),
@@ -586,13 +599,11 @@
             dma((TP,)),
         ],
         compiler_params=pltpu.CompilerParams(
-            collective_id=0, has_side_effects=True, vmem_limit_bytes=vmem_bytes
+            collective_id=0, has_side_effects=True, vmem_limit_bytes=vmem_bytes - 5 * out_bytes // 4
         ),
         name="handover",
     )(payload, *weights, *shared)
-    mixed = results[0]
-    whole = [r.reshape(G, 1, H, C) for r in results[1:4]]
-    return (mixed, *whole, *results[4:])
+    return emit(results, G)
 
 
 def line_length(mesh):

time: 207 us -> 197 us (0.952)
  local copies, waits for them, and re-layouts: 14.6 us -> 1.77 us
  Pallas kernels: 180 us -> 183 us
    unnamed x28 -> x11, local copies, waits for them, and re-layouts: 14.5 us -> 1.66 us
    pallas_call x1 -> x2, Pallas kernels: 180 us -> 183 us  [the longest x1 179 us: body(): pl.pallas_call(functools.partial(handover, dims), out_shape=[pltpu.VMEM((...]
where the time goes in v1:
time: 197 us; the launch traced here: 196 us
  Pallas kernels  183 us (93%)
  other arithmetic  11 us (6%)
    pallas_call x1, Pallas kernels, body(): pl.pallas_call(functools.partial(handover, dims), out_shape=[pltpu.VMEM((...  179 us

profile of v1, /device:TPU:1, one launch (start us, length us, event | category | flops | bytes accessed | tf_op | source)
XLA Modules:
  0.0 196.3 jit_solution(2382882722143043794)
XLA Ops:
  0.6 0.0 copy-start.1
  0.7 1.5 multiply_reduce_fusion
  2.1 0.7 reduce_sum.28
  2.9 0.7 divide_multiply_fusion
  3.6 0.1 copy.20
  3.7 0.8 copy.19
  4.5 0.4 select_reduce_fusion
  5.0 0.0 copy-start
  5.0 1.7 convert_element_type.41.s2
  6.7 1.8 multiply_convert_fusion.2
  8.5 0.0 copy-done.1
  8.5 0.0 copy-start.3
  8.5 1.1 convert_element_type.38.w2
  9.6 0.0 copy-done
  9.6 0.0 copy-start.2
  9.6 0.1 convert_element_type.32
  9.8 0.1 fusion
  9.9 0.8 pad_maximum_fusion.tok
  10.7 0.0 copy-done.3
  10.7 0.8 copy-done.2
  11.5 0.0 copy-done.4
  11.5 1.9 multiply_convert_fusion
  13.5 179.0 %handover.1 = (bf16[176,1024]{1,0:T(8,128)(2,1)S(1)}, bf16[2,512,1024]{2,1,0:T(8,128)(2,1)S(1)}, bf16[2,512,1024]{2,1,0:T(8,128)(2,1)S(1)}, bf16[2,512,1024]{2,1...) custom-call(bf16[176,1152]{1,0:T(8,128)(2,1)} %pad_maximum_fusion.to, ...), custom_call_target="tpu_custom_call" | custom-call | tf_op jit(solution)/shard_map/handover/pallas_call | solution.py:562
  192.5 3.8 %emit.1 = (bf16[176,1024]{1,0:T(8,128)(2,1)}, bf16[2,1,512,1024]{3,2,1,0:T(8,128)(2,1)}, bf16[2,1,512,1024]{3,2,1,0:T(8,128)(2,1)}, bf16[2,1,512,1024]{3,2,1,0:T...) custom-call(bf16[176,1024]{1,0:T(8,128)(2,1)S(1)} %get-tuple-element.14.refs_0_, ...), custom_call_target="tpu_custom_call" | custom-call | tf_op jit(solution)/shard_map/emit/pallas_call | solution.py:497
  (5 shorter events, 0.0 us)
Async XLA Ops:
  0.6 7.9 %copy-start.1 = (f32[8,64,1024]{2,1,0:T(8,128)S(1)}, f32[8,64,1024]{2,1,0:T(8,128)}, u32[]{:S(2)}) copy-start(f32[8,64,1024]{2,1,0:T(8,128)} %param.16) | copy-start | bytes 6291460
  5.0 4.6 %copy-start = (bf16[176,2048]{1,0:T(8,128)(2,1)S(1)}, bf16[176,2048]{1,0:T(8,128)(2,1)}, u32[]{:S(2)}) copy-start(bf16[176,2048]{1,0:T(8,128)(2,1)} %param.10) | copy-start | bytes 2162692
  8.5 2.2 %copy-start.3 = (f32[8,64,1024]{2,1,0:T(8,128)S(1)}, f32[8,64,1024]{2,1,0:T(8,128)}, u32[]{:S(2)}) copy-start(f32[8,64,1024]{2,1,0:T(8,128)} %param.14) | copy-start | bytes 6291460
  9.6 1.9 copy-start.2
  9.6 1.9 copy-start.4

commit v2 on v1

v2 whole, which is shorter than its diff:
```python
import functools

import jax
import jax.numpy as jnp
from jax import lax
from jax.experimental import pallas as pl
from jax.experimental.pallas import tpu as pltpu
from jax.sharding import PartitionSpec as P

SCHEDULE = ('B', 'T', 'C0', 'X0', 'W0:0:4', 'C1', 'C2', 'c', 'X1', 'X2', 'R1', 'W0:4:8', 'F0:0:4', 'R2', 'W1:0:4', 'F0:4:8', 'R3', 'W1:4:8', 'W2', 'F1', 'S', 'F2:0:4', 'O0', 'O1', 'O2', 'O3', 'M0', 'V0', 'F2:4:8', 'A0', 'A1', 's0', 'M1', 'V1', 's1', 'A2', 'a', 'D0', 's2', 's3', 'G0', 'H', 'P', 'E')
route_scale = 2.5
norm_eps = 1e-06
vmem_bytes = 67043328


def fold_gain(weight, gain):
    return (weight * gain).astype(jnp.bfloat16)


def silu(v):
    return v / (1.0 + jnp.exp(-v))


def handover(
    dims,
    tok,
    ids,
    scores,
    gain,
    w0,
    w1,
    w2,
    s0,
    s1,
    s2,
    mixed,
    n0,
    n1,
    n2,
    h0,
    h1,
    h2,
    tokv,
    wf,
    sf,
    wb,
    xs,
    pout,
    pin,
    act,
    oz,
    rety,
    ret,
    psh,
    pshin,
    in_sem,
    tok_send,
    tok_recv,
    w_send,
    w_recv,
    x_send,
    x_recv,
    sh_send,
    sh_recv,
    shx_send,
    shx_recv,
    p_send,
    p_recv,
    a_send,
    a_recv,
    ry_send,
    ry_recv,
    r_send,
    r_recv,
    ps_send,
    ps_recv,
):
    G, S, TP, T, C, H, F, SF, slots, Y, halves, modes = dims
    Z = S // Y
    E = G * S
    SH = SF * S
    NB = S // TP
    NH = NB * T
    gi, si, ti = lax.axis_index("gr"), lax.axis_index("fs"), lax.axis_index("tp")
    zi, yi = si // Y, lax.rem(si, Y)
    w, new, sh, shn = (w0, w1, w2), (n0, n1, n2), (s0, s1, s2), (h0, h1, h2)
    HW, pieces = C // halves, len(modes)
    CW = C // pieces
    parts = [(0, 0, C), (1, 0, C)] + [(2, h * HW, HW) for h in range(halves)]

    def rdma(src, dst, ssem, rsem, dev):
        return pltpu.make_async_remote_copy(
            src_ref=src,
            dst_ref=dst,
            send_sem=ssem,
            recv_sem=rsem,
            device_id=dev,
            device_id_type=pl.DeviceIdType.MESH,
        )

    def rows(start, step, size):
        return pl.ds(pl.multiple_of(start * step, step), size)

    def each(lo, hi, fn):
        def step(i, c):
            fn(i)
            return c

        lax.fori_loop(lo, hi, step, 0)

    def fs_peer(k):
        return lax.rem(si + k, S)

    def fs_from(k):
        return lax.rem(si + S - k, S)

    def gr_peer(k):
        return lax.rem(gi + k, G)

    def tp_peer(k):
        return lax.rem(ti + k, TP)

    barrier = pltpu.get_barrier_semaphore()

    def greet(axis, peer, n):
        each(
            1,
            n,
            lambda k: pl.semaphore_signal(
                barrier,
                inc=1,
                device_id={axis: peer(k)},
                device_id_type=pl.DeviceIdType.MESH,
            ),
        )

    greet("fs", fs_peer, S)
    greet("gr", gr_peer, G)
    greet("tp", tp_peer, TP)
    inputs = [
        pltpu.make_async_copy(tok, tokv, in_sem.at[0]),
        *(pltpu.make_async_copy(w[m], wf.at[m], in_sem.at[1 + m]) for m in range(3)),
        *(pltpu.make_async_copy(sh[m], sf.at[m], in_sem.at[4 + m]) for m in range(3)),
    ]
    for copy in inputs:
        copy.start()

    def route_codes():
        share = scores[...] / jnp.sum(scores[...], axis=0, keepdims=True) * route_scale
        expert = lax.broadcasted_iota(jnp.int32, (E, T), 0)
        dense = jnp.zeros((E, T), jnp.float32)
        for k in range(ids.shape[0]):
            dense = dense + jnp.where(expert == ids[k : k + 1, :], share[k : k + 1, :], 0.0)
        high = dense.astype(jnp.bfloat16).astype(jnp.float32)
        coded = [high, dense - high]
        if C + 2 * E < xs.shape[1]:
            coded.append(jnp.zeros((xs.shape[1] - C - 2 * E, T), jnp.float32))
        coded = jnp.concatenate(coded, axis=0)
        xs[rows(si, T, T), C:] = coded.T.astype(jnp.bfloat16)

    def normalize():
        def chunk(i):
            at = rows(i, 16, 16)
            x = tokv[at, :].astype(jnp.float32)
            scale = lax.rsqrt(jnp.mean(x * x, axis=1, keepdims=True) + norm_eps)
            mine = tokv[at, rows(ti, C, C)].astype(jnp.float32)
            to = pl.ds(pl.multiple_of(si * T + i * 16, 16), 16)
            xs[to, 0:C] = (mine * scale).astype(jnp.bfloat16)

        each(0, T // 16, chunk)

    def fold(m):
        def one(k):
            d = fs_peer(k)
            value = wf[m, d]
            if m < 2:
                value = value * gain[...]
            value = value.astype(jnp.bfloat16)

            def keep():
                new[m][gi, rows(si, F, F), :] = value

            def away():
                wb[m, d] = value

            pl.when(k == 0)(keep)
            pl.when(k > 0)(away)

        each(0, S, one)

    def fold_shared(m):
        value = sf[m]
        if m < 2:
            value = value * gain[...]
        shn[m][rows(si, SF, SF), :] = value.astype(jnp.bfloat16)

    def w_copy(q, d, s):
        m, c, width = parts[q]
        return rdma(
            wb.at[m, d, :, pl.ds(c, width)],
            new[m].at[gi, rows(s, F, F), pl.ds(c, width)],
            w_send.at[q, d],
            w_recv.at[q, s],
            {"fs": d},
        )

    def spread(block, s, up, down, act_on):
        place, ssem, rsem, after = block
        at = place(s)

        def hop(way, dev):
            act_on(rdma(at, at, ssem.at[s, way], rsem.at[s], {"fs": dev}))

        if up:
            pl.when(zi < Z - 1)(lambda: hop(0, si + Y))
        if down:
            pl.when(zi > 0)(lambda: hop(1, si - Y))

        def across(k):
            y = lax.rem(yi + k, Y)
            hop(2 + y, zi * Y + y)

        each(1, Y, across)

    def shx_copy(m, s, g, dev):
        at = sh_place(m, s, g)
        return rdma(at, at, shx_send.at[m, s, dev], shx_recv.at[m, s, g], {"gr": dev})

    def arrive(block, s):
        place, ssem, rsem, after = block
        rdma(place(s), place(s), ssem.at[s, 0], rsem.at[s], {"fs": fs_peer(1)}).wait_recv()
        if after is not None:
            after(s)

    def start(c):
        c.start()

    def sent(c):
        c.wait_send()

    def relay(block, step, act_on=start):
        def from_below():
            s = si - step * Y
            if act_on is start:
                arrive(block, s)
            spread(block, s, True, False, act_on)

        def from_above():
            s = si + step * Y
            if act_on is start:
                arrive(block, s)
            spread(block, s, False, True, act_on)

        pl.when(zi >= step)(from_below)
        pl.when(zi + step < Z)(from_above)

    def others_arrive(block, step):
        def at(z):
            each(1, Y, lambda k: arrive(block, z * Y + lax.rem(yi + k, Y)))

        if step == 0:
            at(zi)
        else:
            pl.when(zi >= step)(lambda: at(zi - step))
            pl.when(zi + step < Z)(lambda: at(zi + step))

    def block_sent(block):
        spread(block, si, True, True, sent)
        for step in range(1, Z):
            relay(block, step, sent)

    def sh_place(m, s, g):
        return shn[m].at[rows(s, SF, SF), rows(g, C // G, C // G)]

    def sh_block(m):
        return (
            lambda s: sh_place(m, s, gi),
            sh_send.at[m],
            sh_recv.at[m],
            lambda s: each(1, G, lambda j: shx_copy(m, s, gi, gr_peer(j)).start()),
        )

    tok_block = (lambda s: xs.at[rows(s, T, T)], tok_send, tok_recv, None)
    sh_blocks = [sh_block(m) for m in range(3)]

    def sh_hop(block, s, way, dev, act_on):
        place, ssem, rsem, after = block
        act_on(rdma(place(s), place(s), ssem.at[s, way], rsem.at[s], {"fs": dev}))

    def sh_along(block, s, up, down, act_on):
        if up:
            pl.when(zi < Z - 1)(lambda: sh_hop(block, s, 0, si + Y, act_on))
        if down:
            pl.when(zi > 0)(lambda: sh_hop(block, s, 1, si - Y, act_on))

    def sh_own(block, act_on):
        def across(k):
            y = lax.rem(yi + k, Y)
            sh_hop(block, si, 2 + y, zi * Y + y, act_on)

        each(1, Y, across)
        sh_along(block, si, True, True, act_on)

    def sh_relay(block, step, act_on):
        def one(s, up, down):
            if act_on is start:
                arrive(block, s)
            sh_along(block, s, up, down, act_on)

        if step == 0:
            each(1, Y, lambda k: one(zi * Y + lax.rem(yi + k, Y), True, True))
            return

        def row(z, up):
            each(0, Y, lambda k: one(z * Y + lax.rem(yi + k, Y), up, not up))

        pl.when(zi >= step)(lambda: row(zi - step, True))
        pl.when(zi + step < Z)(lambda: row(zi + step, False))

    def sh_sent(block):
        sh_own(block, sent)
        for step in range(Z):
            sh_relay(block, step, sent)

    def x_copy(q, s, g, dev):
        m, c, width = parts[q]
        place = new[m].at[g, rows(s, F, F), pl.ds(c, width)]
        return rdma(place, place, x_send.at[q, s, dev], x_recv.at[q, s, g], {"gr": dev})

    def send_weight(q):
        each(1, S, lambda k: w_copy(q, fs_peer(k), si).start())

    def send_own(q):
        each(1, G, lambda j: x_copy(q, si, gi, gr_peer(j)).start())

    def forward(m, lo=1, hi=S):
        def one(k):
            s = fs_from(k)
            w_copy(m, s, s).wait_recv()
            each(1, G, lambda j: x_copy(m, s, gi, gr_peer(j)).start())

        each(lo, hi, one)

    def x_arrive(m, g):
        each(0, S, lambda s: x_copy(m, s, g, g).wait_recv())

    def p_copy(j, t, s):
        return rdma(
            pout.at[j if slots > 1 else 0, t], pin.at[j, s], p_send.at[j, t], p_recv.at[j, s], {"tp": t}
        )

    def a_copy(j, t, s):
        place = act.at[j, rows(s, NH, NH)]
        return rdma(place, place, a_send.at[j, t], a_recv.at[j, s], {"tp": t})

    def first_matmuls(j):
        g = gr_peer(j)
        slot = j if slots > 1 else 0
        for q in range(TP):
            t = tp_peer(1 + q)

            def block(b, t=t):
                x = xs[rows(t * NB + b, T, T), 0:C]
                for m in range(2):
                    part = lax.dot_general(
                        x, new[m][g], (((1,), (1,)), ((), ())), preferred_element_type=jnp.float32
                    )
                    pout[slot, t, rows(b, T, T), m * H : (m + 1) * H] = part.astype(jnp.bfloat16)

            each(0, NB, block)
            if q < TP - 1:
                p_copy(j, t, ti).start()

    def activations(j):
        g = gr_peer(j)
        slot = j if slots > 1 else 0
        expert = g * S + si
        for q in range(1, TP):
            t = tp_peer(q)
            p_copy(j, t, t).wait_recv()

        def block(b):
            r = rows(b, T, T)
            pre = pout[slot, ti, r, :].astype(jnp.float32)
            for q in range(1, TP):
                pre = pre + pin[j, tp_peer(q), r, :].astype(jnp.float32)
            at = rows(ti * NB + b, T, T)
            coded = xs[at, C:].astype(jnp.float32)
            lane = lax.broadcasted_iota(jnp.int32, coded.shape, 1)
            share = jnp.sum(
                jnp.where((lane == expert) | (lane == expert + E), coded, 0.0), axis=1, keepdims=True
            )
            value = silu(pre[:, :H]) * pre[:, H:] * share
            act[j, at, :] = value.astype(jnp.bfloat16)

        each(0, NB, block)
        for q in range(1, TP):
            a_copy(j, tp_peer(q), ti).start()

    def p_copy(j, t, s, place):
        return rdma(
            pout.at[j if slots > 1 else 0, t],
            pin.at[j, place],
            p_send.at[j, t],
            p_recv.at[j, s],
            {"tp": t},
        )

    def a_copy(j, t, s):
        place = act.at[j, rows(s, NH, NH)]
        return rdma(place, place, a_send.at[j, t], a_recv.at[j, s], {"tp": t})

    PB = 2 if NB % 2 == 0 else 1

    def first_matmuls(j):
        g = gr_peer(j)
        slot = j if slots > 1 else 0
        for q in range(TP):
            t = tp_peer(1 + q)

            def block(b, t=t):
                x = xs[pl.ds(pl.multiple_of((t * NB + b * PB) * T, T), PB * T), 0:C]
                for m in range(2):
                    part = lax.dot_general(
                        x, new[m][g], (((1,), (1,)), ((), ())), preferred_element_type=jnp.float32
                    )
                    at = pl.ds(pl.multiple_of(b * PB * T, T), PB * T)
                    pout[slot, t, at, m * H : (m + 1) * H] = part.astype(jnp.bfloat16)

            each(0, NB // PB, block)
            if q < TP - 1:
                p_copy(j, t, ti, TP - 2 - q).start()

    def activations(j):
        g = gr_peer(j)
        slot = j if slots > 1 else 0
        expert = g * S + si
        for q in range(1, TP):
            t = tp_peer(q)
            p_copy(j, t, t, q - 1).wait_recv()

        def block(b):
            r = rows(b, T, T)
            pre = pout[slot, ti, r, :].astype(jnp.float32)
            for q in range(1, TP):
                pre = pre + pin[j, q - 1, r, :].astype(jnp.float32)
            at = rows(ti * NB + b, T, T)
            coded = xs[at, C:].astype(jnp.float32)
            lane = lax.broadcasted_iota(jnp.int32, coded.shape, 1)
            share = jnp.sum(
                jnp.where((lane == expert) | (lane == expert + E), coded, 0.0), axis=1, keepdims=True
            )
            value = silu(pre[:, :H]) * pre[:, H:] * share
            act[j, at, :] = value.astype(jnp.bfloat16)

        each(0, NB, block)
        for q in range(1, TP):
            a_copy(j, tp_peer(q), ti).start()

    def x_arrive(q, g):
        each(0, S, lambda s: x_copy(q, s, g, g).wait_recv())

    def piece(p):
        return pl.ds(p * CW, CW)

    def ry_copy(p, z, y, src):
        return rdma(
            oz.at[rows(z * Y + y, T, T), piece(p)],
            rety.at[p, z, src],
            ry_send.at[p, z, y],
            ry_recv.at[p, z, src],
            {"fs": zi * Y + y},
        )

    def r_copy(p, z, y, col, up, dist):
        slot = Z if dist == 1 and not up else z
        return rdma(
            oz.at[rows(z * Y + y, T, T), piece(p)],
            ret.at[p, col, slot],
            r_send.at[p, col, z],
            r_recv.at[p, col, slot],
            {"fs": si + Y if up else si - Y},
        )

    def far_first(fn):
        for dist in range(Z - 1, -1, -1):
            pl.when(zi + dist < Z)(functools.partial(fn, zi + dist, True, dist))
            if dist:
                pl.when(zi >= dist)(functools.partial(fn, zi - dist, False, dist))

    def down(p):
        def block(z, up, dist):
            def column(k):
                y = lax.rem(yi + k, Y)
                at = rows(z * Y + y, T, T)
                total = jnp.zeros((T, CW), jnp.float32)
                for j in range(G):
                    total = total + jnp.dot(
                        act[j, at, :], new[2][gr_peer(j), :, piece(p)], preferred_element_type=jnp.float32
                    )
                oz[at, piece(p)] = total.astype(jnp.bfloat16)
                if modes[p] == "A":
                    pl.when(y != yi)(lambda: ry_copy(p, z, y, yi).start())
                elif dist:
                    ends = zi == 0 if up else zi == Z - 1
                    pl.when(ends)(lambda: r_copy(p, z, y, y, up, dist).start())

            each(1, Y + 1, column)

        far_first(block)

    def chain(p, z, y, col, up, dist, final=False):
        at = rows(z * Y + y, T, T)

        def add_far(slot):
            rdma(
                ret.at[p, col, slot],
                ret.at[p, col, slot],
                r_send.at[p, col, z],
                r_recv.at[p, col, slot],
                {"fs": fs_peer(1)},
            ).wait_recv()
            total = oz[at, piece(p)].astype(jnp.float32) + ret[p, col, slot].astype(jnp.float32)
            oz[at, piece(p)] = total.astype(jnp.bfloat16)

        inner = True
        if dist == 0 or up:
            inner = zi > 0
            pl.when(zi > 0)(lambda: add_far(z))
        if dist == 0:
            pl.when(zi < Z - 1)(lambda: add_far(Z))
        elif not up:
            inner = zi < Z - 1
            pl.when(zi < Z - 1)(lambda: add_far(z))
        if dist:
            if modes[p] == "A":
                r_copy(p, z, y, col, up, dist).start()
            else:
                pl.when(inner)(lambda: r_copy(p, z, y, col, up, dist).start())

    def across_sum(p, z):
        at = rows(z * Y + yi, T, T)
        total = oz[at, piece(p)].astype(jnp.float32)
        for k in range(1, Y):
            y = lax.rem(yi + k, Y)
            ry_copy(p, z, y, y).wait_recv()
            total = total + rety[p, z, y].astype(jnp.float32)
        oz[at, piece(p)] = total.astype(jnp.bfloat16)

    def gather_far(p):
        def block(z, up, dist):
            if modes[p] == "A":
                across_sum(p, z)
                chain(p, z, yi, 0, up, dist)
                return

            def column(k):
                y = lax.rem(yi + k, Y)
                chain(p, z, y, y, up, dist)
                if dist == 0:
                    pl.when(y != yi)(lambda: ry_copy(p, z, y, yi).start())

            each(1, Y + 1, column)

        far_first(block)

    def gather_near(p):
        if modes[p] == "B":
            across_sum(p, zi)

    def return_sent(p):
        def block(z, up, dist):
            def column(k):
                y = lax.rem(yi + k, Y)
                if modes[p] == "A":
                    pl.when(y != yi)(lambda: ry_copy(p, z, y, yi).wait_send())
                    if dist:
                        pl.when(y == yi)(lambda: r_copy(p, z, y, 0, up, dist).wait_send())
                elif dist:
                    r_copy(p, z, y, y, up, dist).wait_send()
                else:
                    pl.when(y != yi)(lambda: ry_copy(p, z, y, yi).wait_send())

            each(1, Y + 1, column)

        far_first(block)

    def shared_arrive(m):
        each(
            1,
            S,
            lambda k: each(
                1, G, lambda j: shx_copy(m, fs_from(k), gr_peer(j), gr_peer(j)).wait_recv()
            ),
        )

    def ps_copy(t, s):
        return rdma(psh, pshin.at[s], ps_send.at[t], ps_recv.at[s], {"tp": t})

    def shared_first(m):
        part = lax.dot_general(
            xs[rows(si, T, T), 0:C],
            shn[m][...],
            (((1,), (1,)), ((), ())),
            preferred_element_type=jnp.float32,
        )
        psh[:, m * SH : (m + 1) * SH] = part.astype(jnp.bfloat16)

    def act_arrive():
        for q in range(1, TP):
            for j in range(G):
                a_copy(j, tp_peer(q), tp_peer(q)).wait_recv()

    scope = jax.named_scope

    def span(text):
        q, lo, hi = (text + ":0:8").split(":")[:3]
        return int(q), max(1, int(lo) * S // 8), int(hi) * S // 8

    def run(name):
        op, num = name[0], name[1:]
        with scope(name.replace(":", "_")):
            if op == "T":
                spread(tok_block, si, True, True, start)
            elif op == "B":
                pl.semaphore_wait(barrier, S + G + TP - 3)
            elif op == "C":
                m = int(num)
                inputs[1 + m].wait()
                fold(m)
            elif op == "c":
                for m in range(3):
                    inputs[4 + m].wait()
                    fold_shared(m)
            elif op == "X":
                send_own(int(num))
            elif op == "W":
                q, lo, hi = span(num)
                each(lo, hi, lambda k: w_copy(q, fs_peer(k), si).start())
            elif op == "R":
                relay(tok_block, int(num))
            elif op == "F":
                forward(*span(num))
            elif op == "O":
                others_arrive(tok_block, int(num))
            elif op == "S":
                for block in sh_blocks:
                    sh_own(block, start)
            elif op == "s":
                for block in sh_blocks:
                    sh_relay(block, int(num), start)
            elif op == "M":
                j = int(num)
                if slots == 1 and j > 0:
                    for q in range(1, TP):
                        p_copy(j - 1, tp_peer(q), ti, 0).wait_send()
                first_matmuls(j)
            elif op == "V":
                activations(int(num))
            elif op == "A":
                for j in range(1, G):
                    x_arrive(int(num), gr_peer(j))
            elif op == "a":
                act_arrive()
            elif op == "D":
                down(int(num))
            elif op == "G":
                gather_far(int(num))
            elif op == "H":
                for m in range(2):
                    shared_arrive(m)
                    shared_first(m)
                for q in range(1, TP):
                    ps_copy(tp_peer(q), ti).start()
            elif op == "P":
                shared_arrive(2)
                pre = psh[...].astype(jnp.float32)
                for q in range(1, TP):
                    t = tp_peer(q)
                    ps_copy(t, t).wait_recv()
                    pre = pre + pshin[t].astype(jnp.float32)
                shared_act = (silu(pre[:, :SH]) * pre[:, SH:]).astype(jnp.bfloat16)
                rest.append(jnp.dot(shared_act, shn[2][...], preferred_element_type=jnp.float32))
            elif op == "E":
                for p in range(pieces):
                    gather_near(p)
                total = rest[0] + oz[rows(si, T, T), :].astype(jnp.float32)
                mixed[...] = total.astype(jnp.bfloat16)
            else:
                raise ValueError(name)

    rest = []
    with scope("prologue"):
        route_codes()
        inputs[0].wait()
        normalize()
    for name in SCHEDULE:
        run(name)

    for q in range(len(parts)):
        each(1, S, lambda k, q=q: w_copy(q, fs_peer(k), si).wait_send())
        each(0, S, lambda s, q=q: each(1, G, lambda j: x_copy(q, s, gi, gr_peer(j)).wait_send()))
    for m in range(3):
        sh_sent(sh_blocks[m])
        each(
            1,
            S,
            lambda k, m=m: each(
                1, G, lambda j: shx_copy(m, fs_from(k), gi, gr_peer(j)).wait_send()
            ),
        )
    block_sent(tok_block)
    for p in range(pieces):
        return_sent(p)
    for q in range(1, TP):
        t = tp_peer(q)
        ps_copy(t, ti).wait_send()
        for j in range(G):
            if slots > 1 or j == G - 1:
                p_copy(j, t, ti, 0).wait_send()
            a_copy(j, t, ti).wait_send()


def emit_kernel(*refs):
    n = len(refs) // 2
    sem = refs[-1]
    copies = []
    for i in range(n):
        dst = refs[n + i]
        if len(dst.shape) == 4:
            dst = dst.at[:, 0]
        copies.append(pltpu.make_async_copy(refs[i], dst, sem.at[i]))
    for c in copies:
        c.start()
    for c in copies:
        c.wait()


def emit(results, G):
    bf16 = jnp.bfloat16
    shapes = [r.shape if len(r.shape) < 3 else (r.shape[0], 1) + r.shape[1:] for r in results]
    n = len(results)
    return pl.pallas_call(
        emit_kernel,
        out_shape=[jax.ShapeDtypeStruct(s, bf16) for s in shapes],
        in_specs=[pl.BlockSpec(memory_space=pltpu.VMEM)] * n,
        out_specs=[pl.BlockSpec(memory_space=pl.ANY)] * n,
        scratch_shapes=[pltpu.SemaphoreType.DMA((n,))],
        compiler_params=pltpu.CompilerParams(vmem_limit_bytes=vmem_bytes // 2),
        name="emit",
    )(*results)


def body(
    Y,
    tokens,
    expert_ids,
    route_weight,
    norm_gain,
    expert_gate,
    expert_up,
    expert_down,
    shared_gate,
    shared_up,
    shared_down,
):
    G, S, TP = lax.axis_size("gr"), lax.axis_size("fs"), lax.axis_size("tp")
    T, C = tokens.shape[0], expert_gate.shape[2]
    F, SF = expert_gate.shape[1], shared_gate.shape[0]
    H, SH = F * S, SF * S
    E, N = G * S, S * T
    NH = N // TP
    lanes = -(-2 * E // 128) * 128
    bf16, f32 = jnp.bfloat16, jnp.float32
    halves = 1 if C % 256 == 0 and C >= 1024 else 1
    modes = "A" if C % 512 == 0 and C >= 1024 else "A"
    P = len(modes)
    columns = Y if "B" in modes else 1
    Q = 2 + halves

    out_bytes = 2 * C * (T + 3 * G * H + 3 * SH)
    limit = vmem_bytes - 5 * out_bytes // 4
    fixed = 2 * (N * (3 * C + lanes + G * H) + T * (columns * (S // Y + 1) * C + 2 * SH * (TP + 1)))
    fixed += 6 * 3 * S * F * C + 4 * 3 * SF * C + 2 * T * tokens.shape[1] + 2 * N * G * 2 * H
    slots = G if fixed + 2 * N * G * 2 * H < limit - (1 << 21) else 1
    dims = (G, S, TP, T, C, H, F, SF, slots, Y, halves, modes)
    vmem, hbm = pl.BlockSpec(memory_space=pltpu.VMEM), pl.BlockSpec(memory_space=pl.ANY)
    dma = pltpu.SemaphoreType.DMA
    results = pl.pallas_call(
        functools.partial(handover, dims),
        out_shape=[pltpu.VMEM((T, C), bf16)]
        + [pltpu.VMEM((G, H, C), bf16)] * 3
        + [pltpu.VMEM((SH, C), bf16)] * 3,
        in_specs=[hbm, vmem, vmem, vmem] + [hbm] * 6,
        out_specs=[vmem] * 7,
        scratch_shapes=[
            pltpu.VMEM(tokens.shape, bf16),
            pltpu.VMEM((3, S, F, C), f32),
            pltpu.VMEM((3, SF, C), f32),
            pltpu.VMEM((3, S, F, C), bf16),
            pltpu.VMEM((N, C + lanes), bf16),
            pltpu.VMEM((slots, TP, NH, 2 * H), bf16),
            pltpu.VMEM((G, max(TP - 1, 1), NH, 2 * H), bf16),
            pltpu.VMEM((G, N, H), bf16),
            pltpu.VMEM((N, C), bf16),
            pltpu.VMEM((P, S // Y, Y, T, C // P), bf16),
            pltpu.VMEM((P, columns, S // Y + 1, T, C // P), bf16),
            pltpu.VMEM((T, 2 * SH), bf16),
            pltpu.VMEM((TP, T, 2 * SH), bf16),
            dma((7,)),
            dma((S, 2 + Y)),
            dma((S,)),
            dma((Q, S)),
            dma((Q, S)),
            dma((Q, S, G)),
            dma((Q, S, G)),
            dma((3, S, 2 + Y)),
            dma((3, S)),
            dma((3, S, G)),
            dma((3, S, G)),
            dma((G, TP)),
            dma((G, TP)),
            dma((G, TP)),
            dma((G, TP)),
            dma((P, S // Y, Y)),
            dma((P, S // Y, Y)),
            dma((P, columns, S // Y)),
            dma((P, columns, S // Y + 1)),
            dma((TP,)),
            dma((TP,)),
        ],
        compiler_params=pltpu.CompilerParams(
            collective_id=0, has_side_effects=True, vmem_limit_bytes=limit
        ),
        name="handover",
    )(
        tokens,
        expert_ids.T,
        route_weight.T,
        norm_gain[None],
        expert_gate,
        expert_up,
        expert_down,
        shared_gate,
        shared_up,
        shared_down,
    )
    return emit(results, G)


def line_length(mesh):
    places = [d.coords for d in mesh.devices[0, :, 0]]
    axis = [i for i in range(3) if places[0][i] != places[1][i]][0]
    count = 0
    for place in places:
        if any(place[i] != places[0][i] for i in range(3) if i != axis):
            break
        count += 1
    return count if len(places) % count == 0 else len(places)


def solution(mesh):
    placed = (
        P(("gr", "fs"), None),
        P(("gr", "fs"), None),
        P(("gr", "fs"), None),
        P("tp"),
        P("gr", "fs", "tp"),
        P("gr", "fs", "tp"),
        P("gr", "fs", "tp"),
        P("fs", "tp"),
        P("fs", "tp"),
        P("fs", "tp"),
    )
    return jax.shard_map(
        functools.partial(body, line_length(mesh)),
        mesh=mesh,
        in_specs=placed,
        out_specs=(
            P(("gr", "fs"), "tp"),
            P(None, "fs", None, "tp"),
            P(None, "fs", None, "tp"),
            P(None, "fs", None, "tp"),
            P(None, "tp"),
            P(None, "tp"),
            P(None, "tp"),
        ),
        check_vma=False,
    )
```

time: 197 us -> 163 us (0.83)
  Pallas kernels: 183 us -> 161 us
  other arithmetic: 11 us -> 0 us
    pallas_call x1, Pallas kernels: 179 us -> 158 us  [body(): pl.pallas_call(functools.partial(handover, dims), out_shape=[pltpu.VMEM((...]
    convert_element_type x6 -> x0, other arithmetic: 6.8 us -> none  [the longest x2 3.72 us: fold_gain(): return (weight * gain).astype(jnp.bfloat16)]
    reduce_sum x3 -> x0, other arithmetic: 2.65 us -> none  [the longest x1 1.48 us: body(): jnp.mean(tok_float * tok_float, axis=1, keepdims=True) + norm_eps]
where the time goes in v2:
time: 163 us; the launch traced here: 162 us
  Pallas kernels  161 us (99%)
    pallas_call x1, Pallas kernels, body(): pl.pallas_call(functools.partial(handover, dims), out_shape=[pltpu.VMEM((...  158 us
    pallas_call x1, Pallas kernels, emit(): pl.pallas_call(emit_kernel, out_shape=[jax.ShapeDtypeStruct(s, bf16) for...  3.8 us

profile of v2, /device:TPU:1, one launch (start us, length us, event | category | flops | bytes accessed | tf_op | source)
XLA Modules:
  0.0 162.0 jit_solution(11125940050291874358)
XLA Ops:
  0.6 157.6 %handover.1 = (bf16[176,1024]{1,0:T(8,128)(2,1)S(1)}, bf16[2,512,1024]{2,1,0:T(8,128)(2,1)S(1)}, bf16[2,512,1024]{2,1,0:T(8,128)(2,1)S(1)}, bf16[2,512,1024]{2,1...) custom-call(bf16[176,2048]{1,0:T(8,128)(2,1)} %tok.1, ...), custom_call_target="tpu_custom_call" | custom-call | tf_op jit(solution)/shard_map/handover/pallas_call | solution.py:789
  158.2 3.8 %emit.1 = (bf16[176,1024]{1,0:T(8,128)(2,1)}, bf16[2,1,512,1024]{3,2,1,0:T(8,128)(2,1)}, bf16[2,1,512,1024]{3,2,1,0:T(8,128)(2,1)}, bf16[2,1,512,1024]{3,2,1,0:T...) custom-call(bf16[176,1024]{1,0:T(8,128)(2,1)S(1)} %get-tuple-element.14.refs_0_, ...), custom_call_target="tpu_custom_call" | custom-call | tf_op jit(solution)/shard_map/emit/pallas_call | solution.py:743

commit v3 on v2

--- a/solution.py
+++ b/solution.py
@@ -7,7 +7,7 @@
 from jax.experimental.pallas import tpu as pltpu
 from jax.sharding import PartitionSpec as P
 
-SCHEDULE = ('B', 'T', 'C0', 'X0', 'W0:0:4', 'C1', 'C2', 'c', 'X1', 'X2', 'R1', 'W0:4:8', 'F0:0:4', 'R2', 'W1:0:4', 'F0:4:8', 'R3', 'W1:4:8', 'W2', 'F1', 'S', 'F2:0:4', 'O0', 'O1', 'O2', 'O3', 'M0', 'V0', 'F2:4:8', 'A0', 'A1', 's0', 'M1', 'V1', 's1', 'A2', 'a', 'D0', 's2', 's3', 'G0', 'H', 'P', 'E')
+SCHEDULE = ('B', 'T', 'C0', 'X0', 'W001', 'C1', 'C2', 'c', 'X1', 'X2', 'W10', 'W20', 'R1', 'W023', 'F00', 'F01', 'F10', 'F20', 'R2', 'W11', 'F02', 'F03', 'R3', 'W123', 'F11', 'W2123', 'F12', 'F13', 'S', 'O0', 'O1', 'O2', 'O3', 'M0', 'F21', 'F22', 'F23', 'V0', 'A0', 'A1', 's0', 'M1', 'V1', 's1', 'A2', 'a', 'D0', 's2', 'G0:3', 'wT01', 's3', 'G0:2', 'w2Ps', 'G0:1', 'H', 'P', 'wS', 'G0:0', 'E', 'wRp')
 route_scale = 2.5
 norm_eps = 1e-06
 vmem_bytes = 67043328
@@ -37,9 +37,7 @@
     n0,
     n1,
     n2,
-    h0,
-    h1,
-    h2,
+    hs,
     tokv,
     wf,
     sf,
@@ -83,7 +81,7 @@
     NH = NB * T
     gi, si, ti = lax.axis_index("gr"), lax.axis_index("fs"), lax.axis_index("tp")
     zi, yi = si // Y, lax.rem(si, Y)
-    w, new, sh, shn = (w0, w1, w2), (n0, n1, n2), (s0, s1, s2), (h0, h1, h2)
+    w, new, sh = (w0, w1, w2), (n0, n1, n2), (s0, s1, s2)
     HW, pieces = C // halves, len(modes)
     CW = C // pieces
     parts = [(0, 0, C), (1, 0, C)] + [(2, h * HW, HW) for h in range(halves)]
@@ -192,14 +190,14 @@
         value = sf[m]
         if m < 2:
             value = value * gain[...]
-        shn[m][rows(si, SF, SF), :] = value.astype(jnp.bfloat16)
+        hs[m, rows(si, SF, SF), :] = value.astype(jnp.bfloat16)
 
     def w_copy(q, d, s):
         m, c, width = parts[q]
         return rdma(
             wb.at[m, d, :, pl.ds(c, width)],
             new[m].at[gi, rows(s, F, F), pl.ds(c, width)],
-            w_send.at[q, d],
+            w_send.at[q],
             w_recv.at[q, s],
             {"fs": d},
         )
@@ -222,9 +220,12 @@
 
         each(1, Y, across)
 
-    def shx_copy(m, s, g, dev):
-        at = sh_place(m, s, g)
-        return rdma(at, at, shx_send.at[m, s, dev], shx_recv.at[m, s, g], {"gr": dev})
+    def sh_place(s, g):
+        return hs.at[:, rows(s, SF, SF), rows(g, C // G, C // G)]
+
+    def shx_copy(s, g, dev):
+        at = sh_place(s, g)
+        return rdma(at, at, shx_send.at[dev], shx_recv.at[g], {"gr": dev})
 
     def arrive(block, s):
         place, ssem, rsem, after = block
@@ -269,19 +270,13 @@
         for step in range(1, Z):
             relay(block, step, sent)
 
-    def sh_place(m, s, g):
-        return shn[m].at[rows(s, SF, SF), rows(g, C // G, C // G)]
-
-    def sh_block(m):
-        return (
-            lambda s: sh_place(m, s, gi),
-            sh_send.at[m],
-            sh_recv.at[m],
-            lambda s: each(1, G, lambda j: shx_copy(m, s, gi, gr_peer(j)).start()),
-        )
-
+    sh_block = (
+        lambda s: sh_place(s, gi),
+        sh_send,
+        sh_recv,
+        lambda s: each(1, G, lambda j: shx_copy(s, gi, gr_peer(j)).start()),
+    )
     tok_block = (lambda s: xs.at[rows(s, T, T)], tok_send, tok_recv, None)
-    sh_blocks = [sh_block(m) for m in range(3)]
 
     def sh_hop(block, s, way, dev, act_on):
         place, ssem, rsem, after = block
@@ -325,24 +320,10 @@
     def x_copy(q, s, g, dev):
         m, c, width = parts[q]
         place = new[m].at[g, rows(s, F, F), pl.ds(c, width)]
-        return rdma(place, place, x_send.at[q, s, dev], x_recv.at[q, s, g], {"gr": dev})
-
-    def send_weight(q):
-        each(1, S, lambda k: w_copy(q, fs_peer(k), si).start())
+        return rdma(place, place, x_send.at[q, dev], x_recv.at[q, g], {"gr": dev})
 
     def send_own(q):
         each(1, G, lambda j: x_copy(q, si, gi, gr_peer(j)).start())
-
-    def forward(m, lo=1, hi=S):
-        def one(k):
-            s = fs_from(k)
-            w_copy(m, s, s).wait_recv()
-            each(1, G, lambda j: x_copy(m, s, gi, gr_peer(j)).start())
-
-        each(lo, hi, one)
-
-    def x_arrive(m, g):
-        each(0, S, lambda s: x_copy(m, s, g, g).wait_recv())
 
     def p_copy(j, t, s):
         return rdma(
@@ -457,8 +438,13 @@
         for q in range(1, TP):
             a_copy(j, tp_peer(q), ti).start()
 
+    def x_whole(q, g, dev):
+        m, c, width = parts[q]
+        place = new[m].at[g, :, pl.ds(c, width)]
+        return rdma(place, place, x_send.at[q, dev], x_recv.at[q, g], {"gr": dev})
+
     def x_arrive(q, g):
-        each(0, S, lambda s: x_copy(q, s, g, g).wait_recv())
+        x_whole(q, g, g).wait_recv()
 
     def piece(p):
         return pl.ds(p * CW, CW)
@@ -482,8 +468,10 @@
             {"fs": si + Y if up else si - Y},
         )
 
-    def far_first(fn):
+    def far_first(fn, only=None):
         for dist in range(Z - 1, -1, -1):
+            if only is not None and dist != only:
+                continue
             pl.when(zi + dist < Z)(functools.partial(fn, zi + dist, True, dist))
             if dist:
                 pl.when(zi >= dist)(functools.partial(fn, zi - dist, False, dist))
@@ -547,7 +535,7 @@
             total = total + rety[p, z, y].astype(jnp.float32)
         oz[at, piece(p)] = total.astype(jnp.bfloat16)
 
-    def gather_far(p):
+    def gather_far(p, only=None):
         def block(z, up, dist):
             if modes[p] == "A":
                 across_sum(p, z)
@@ -562,7 +550,7 @@
 
             each(1, Y + 1, column)
 
-        far_first(block)
+        far_first(block, only)
 
     def gather_near(p):
         if modes[p] == "B":
@@ -585,14 +573,12 @@
 
         far_first(block)
 
-    def shared_arrive(m):
-        each(
-            1,
-            S,
-            lambda k: each(
-                1, G, lambda j: shx_copy(m, fs_from(k), gr_peer(j), gr_peer(j)).wait_recv()
-            ),
-        )
+    def shx_whole(g, dev):
+        at = hs.at[:, pl.ds(0, SH - SF), rows(g, C // G, C // G)]
+        return rdma(at, at, shx_send.at[dev], shx_recv.at[g], {"gr": dev})
+
+    def shared_arrive():
+        each(1, G, lambda j: shx_whole(gr_peer(j), gr_peer(j)).wait_recv())
 
     def ps_copy(t, s):
         return rdma(psh, pshin.at[s], ps_send.at[t], ps_recv.at[s], {"tp": t})
@@ -600,7 +586,7 @@
     def shared_first(m):
         part = lax.dot_general(
             xs[rows(si, T, T), 0:C],
-            shn[m][...],
+            hs[m],
             (((1,), (1,)), ((), ())),
             preferred_element_type=jnp.float32,
         )
@@ -613,9 +599,54 @@
 
     scope = jax.named_scope
 
-    def span(text):
-        q, lo, hi = (text + ":0:8").split(":")[:3]
-        return int(q), max(1, int(lo) * S // 8), int(hi) * S // 8
+    def peers(order, fn):
+        for dist in (int(v) for v in order):
+            if dist == 0:
+                each(1, Y, lambda k: fn(zi * Y + lax.rem(yi + k, Y)))
+            elif dist < Z:
+
+                def row(z):
+                    each(0, Y, lambda k: fn(z * Y + lax.rem(yi + k, Y)))
+
+                pl.when(zi + dist < Z)(lambda dist=dist: row(zi + dist))
+                pl.when(zi >= dist)(lambda dist=dist: row(zi - dist))
+
+    def weight_out(q, order):
+        peers(order, lambda d: w_copy(q, d, si).start())
+
+    def weight_on(q, order):
+        def one(s):
+            w_copy(q, s, s).wait_recv()
+            each(1, G, lambda j: x_copy(q, s, gi, gr_peer(j)).start())
+
+        peers(order, one)
+
+    def settle(kind):
+        if kind == "T":
+            block_sent(tok_block)
+        elif kind == "S":
+            sh_sent(sh_block)
+        elif kind == "s":
+            each(1, G, lambda j: shx_whole(gi, gr_peer(j)).wait_send())
+        elif kind == "R":
+            for p in range(pieces):
+                return_sent(p)
+        elif kind == "P":
+            for q in range(1, TP):
+                t = tp_peer(q)
+                for j in range(G):
+                    if slots > 1 or j == G - 1:
+                        p_copy(j, t, ti, 0).wait_send()
+                    a_copy(j, t, ti).wait_send()
+        elif kind == "p":
+            for q in range(1, TP):
+                ps_copy(tp_peer(q), ti).wait_send()
+        else:
+            q = int(kind)
+            m, c, width = parts[q]
+            away = wb.at[m, pl.ds(0, S - 1), :, pl.ds(c, width)]
+            rdma(away, away, w_send.at[q], w_recv.at[q, si], {"fs": fs_peer(1)}).wait_send()
+            each(1, G, lambda j: x_whole(q, gi, gr_peer(j)).wait_send())
 
     def run(name):
         op, num = name[0], name[1:]
@@ -635,20 +666,17 @@
             elif op == "X":
                 send_own(int(num))
             elif op == "W":
-                q, lo, hi = span(num)
-                each(lo, hi, lambda k: w_copy(q, fs_peer(k), si).start())
+                weight_out(int(num[0]), num[1:])
             elif op == "R":
                 relay(tok_block, int(num))
             elif op == "F":
-                forward(*span(num))
+                weight_on(int(num[0]), num[1:])
             elif op == "O":
                 others_arrive(tok_block, int(num))
             elif op == "S":
-                for block in sh_blocks:
-                    sh_own(block, start)
+                sh_own(sh_block, start)
             elif op == "s":
-                for block in sh_blocks:
-                    sh_relay(block, int(num), start)
+                sh_relay(sh_block, int(num), start)
             elif op == "M":
                 j = int(num)
                 if slots == 1 and j > 0:
@@ -665,27 +693,29 @@
             elif op == "D":
                 down(int(num))
             elif op == "G":
-                gather_far(int(num))
+                gather_far(*(int(v) for v in num.split(":")))
             elif op == "H":
+                shared_arrive()
                 for m in range(2):
-                    shared_arrive(m)
                     shared_first(m)
                 for q in range(1, TP):
                     ps_copy(tp_peer(q), ti).start()
             elif op == "P":
-                shared_arrive(2)
                 pre = psh[...].astype(jnp.float32)
                 for q in range(1, TP):
                     t = tp_peer(q)
                     ps_copy(t, t).wait_recv()
                     pre = pre + pshin[t].astype(jnp.float32)
                 shared_act = (silu(pre[:, :SH]) * pre[:, SH:]).astype(jnp.bfloat16)
-                rest.append(jnp.dot(shared_act, shn[2][...], preferred_element_type=jnp.float32))
+                rest.append(jnp.dot(shared_act, hs[2], preferred_element_type=jnp.float32))
             elif op == "E":
                 for p in range(pieces):
                     gather_near(p)
                 total = rest[0] + oz[rows(si, T, T), :].astype(jnp.float32)
                 mixed[...] = total.astype(jnp.bfloat16)
+            elif op == "w":
+                for kind in num:
+                    settle(kind)
             else:
                 raise ValueError(name)
 
@@ -697,55 +727,29 @@
     for name in SCHEDULE:
         run(name)
 
-    for q in range(len(parts)):
-        each(1, S, lambda k, q=q: w_copy(q, fs_peer(k), si).wait_send())
-        each(0, S, lambda s, q=q: each(1, G, lambda j: x_copy(q, s, gi, gr_peer(j)).wait_send()))
-    for m in range(3):
-        sh_sent(sh_blocks[m])
-        each(
-            1,
-            S,
-            lambda k, m=m: each(
-                1, G, lambda j: shx_copy(m, fs_from(k), gi, gr_peer(j)).wait_send()
-            ),
-        )
-    block_sent(tok_block)
-    for p in range(pieces):
-        return_sent(p)
-    for q in range(1, TP):
-        t = tp_peer(q)
-        ps_copy(t, ti).wait_send()
-        for j in range(G):
-            if slots > 1 or j == G - 1:
-                p_copy(j, t, ti, 0).wait_send()
-            a_copy(j, t, ti).wait_send()
-
-
-def emit_kernel(*refs):
-    n = len(refs) // 2
+
+def emit_kernel(mixed, n0, n1, n2, hs, *refs):
     sem = refs[-1]
+    sources = [mixed, n0, n1, n2, hs.at[0], hs.at[1], hs.at[2]]
     copies = []
-    for i in range(n):
-        dst = refs[n + i]
-        if len(dst.shape) == 4:
-            dst = dst.at[:, 0]
-        copies.append(pltpu.make_async_copy(refs[i], dst, sem.at[i]))
-    for c in copies:
-        c.start()
-    for c in copies:
-        c.wait()
-
-
-def emit(results, G):
-    bf16 = jnp.bfloat16
-    shapes = [r.shape if len(r.shape) < 3 else (r.shape[0], 1) + r.shape[1:] for r in results]
-    n = len(results)
+    for i, (src, dst) in enumerate(zip(sources, refs[:-1])):
+        copies.append(pltpu.make_async_copy(src, dst.at[:, 0] if 0 < i < 4 else dst, sem.at[i]))
+    for copy in copies:
+        copy.start()
+    for copy in copies:
+        copy.wait()
+
+
+def emit(results):
+    mixed, whole, shared = results[0], results[1], results[4]
+    G, H, C = whole.shape
+    shapes = [mixed.shape] + [(G, 1, H, C)] * 3 + [shared.shape[1:]] * 3
     return pl.pallas_call(
         emit_kernel,
-        out_shape=[jax.ShapeDtypeStruct(s, bf16) for s in shapes],
-        in_specs=[pl.BlockSpec(memory_space=pltpu.VMEM)] * n,
-        out_specs=[pl.BlockSpec(memory_space=pl.ANY)] * n,
-        scratch_shapes=[pltpu.SemaphoreType.DMA((n,))],
+        out_shape=[jax.ShapeDtypeStruct(s, jnp.bfloat16) for s in shapes],
+        in_specs=[pl.BlockSpec(memory_space=pltpu.VMEM)] * len(results),
+        out_specs=[pl.BlockSpec(memory_space=pl.ANY)] * len(shapes),
+        scratch_shapes=[pltpu.SemaphoreType.DMA((len(shapes),))],
         compiler_params=pltpu.CompilerParams(vmem_limit_bytes=vmem_bytes // 2),
         name="emit",
     )(*results)
@@ -790,9 +794,9 @@
         functools.partial(handover, dims),
         out_shape=[pltpu.VMEM((T, C), bf16)]
         + [pltpu.VMEM((G, H, C), bf16)] * 3
-        + [pltpu.VMEM((SH, C), bf16)] * 3,
+        + [pltpu.VMEM((3, SH, C), bf16)],
         in_specs=[hbm, vmem, vmem, vmem] + [hbm] * 6,
-        out_specs=[vmem] * 7,
+        out_specs=[vmem] * 5,
         scratch_shapes=[
             pltpu.VMEM(tokens.shape, bf16),
             pltpu.VMEM((3, S, F, C), f32),
@@ -810,14 +814,14 @@
             dma((7,)),
             dma((S, 2 + Y)),
             dma((S,)),
+            dma((Q,)),
             dma((Q, S)),
-            dma((Q, S)),
-            dma((Q, S, G)),
-            dma((Q, S, G)),
-            dma((3, S, 2 + Y)),
-            dma((3, S)),
-            dma((3, S, G)),
-            dma((3, S, G)),
+            dma((Q, G)),
+            dma((Q, G)),
+            dma((S, 2 + Y)),
+            dma((S,)),
+            dma((G,)),
+            dma((G,)),
             dma((G, TP)),
             dma((G, TP)),
             dma((G, TP)),
@@ -845,7 +849,7 @@
         shared_up,
         shared_down,
     )
-    return emit(results, G)
+    return emit(results)
 
 
 def line_length(mesh):

time: 163 us -> 147 us (0.902)
  the two profiles are of different devices: /device:TPU:1 before, /device:TPU:12 now
where the time goes in v3:
time: 147 us
  Pallas kernels  146 us (99%)
    pallas_call x1, Pallas kernels, body(): pl.pallas_call(functools.partial(handover, dims), out_shape=[pltpu.VMEM((...  142 us
    pallas_call x1, Pallas kernels, emit(): pl.pallas_call(emit_kernel, out_shape=[jax.ShapeDtypeStruct(s, jnp.bfloat...  3.8 us

profile of v3, /device:TPU:12, one launch (start us, length us, event | category | flops | bytes accessed | tf_op | source)
XLA Modules:
  0.0 146.9 jit_solution(6962744379277481115)
XLA Ops:
  0.6 142.4 %handover.1 = (bf16[176,1024]{1,0:T(8,128)(2,1)S(1)}, bf16[2,512,1024]{2,1,0:T(8,128)(2,1)S(1)}, bf16[2,512,1024]{2,1,0:T(8,128)(2,1)S(1)}, bf16[2,512,1024]{2,1,0:T(8,128)(2,1)S(1)}, bf16[3,512,1024]{2,1,0:T(8,128)(2,1)S(1)}) custom-call(bf16[176,2048]{1,0:T(8,128)(2,1)} %tok.1, s32[8,176]{1,0:T(8,128)} %bitcast.3, f32[8,176]{1,0:T(8,128)} %bitcast.4, ...), custom_call_target="tpu_custom_call" | custom-call | tf_op jit(solution)/shard_map/handover/pallas_call | solution.py:793
  143.1 3.8 %emit.1 = (bf16[176,1024]{1,0:T(8,128)(2,1)}, bf16[2,1,512,1024]{3,2,1,0:T(8,128)(2,1)}, bf16[2,1,512,1024]{3,2,1,0:T(8,128)(2,1)}, bf16[2,1,512,1024]{3,2,1,0:T...) custom-call(bf16[176,1024]{1,0:T(8,128)(2,1)S(1)} %get-tuple-element.12.mixed, ...), custom_call_target="tpu_custom_call" | custom-call | tf_op jit(solution)/shard_map/emit/pallas_call | solution.py:747

commit v4 on v3

--- a/solution.py
+++ b/solution.py
@@ -7,7 +7,13 @@
 from jax.experimental.pallas import tpu as pltpu
 from jax.sharding import PartitionSpec as P
 
-SCHEDULE = ('B', 'T', 'C0', 'X0', 'W001', 'C1', 'C2', 'c', 'X1', 'X2', 'W10', 'W20', 'R1', 'W023', 'F00', 'F01', 'F10', 'F20', 'R2', 'W11', 'F02', 'F03', 'R3', 'W123', 'F11', 'W2123', 'F12', 'F13', 'S', 'O0', 'O1', 'O2', 'O3', 'M0', 'F21', 'F22', 'F23', 'V0', 'A0', 'A1', 's0', 'M1', 'V1', 's1', 'A2', 'a', 'D0', 's2', 'G0:3', 'wT01', 's3', 'G0:2', 'w2Ps', 'G0:1', 'H', 'P', 'wS', 'G0:0', 'E', 'wRp')
+SCHEDULE = (
+    "B", "T", "C0", "X0", "W001", "C1", "C2", "c", "X1", "X2", "W10", "W20", "R1", "W023", "F00",
+    "F01", "F10", "F20", "R2", "W11", "F02", "F03", "R3", "W123", "F11", "W21", "F12", "W22", "F13",
+    "W23", "O0", "O1", "O2", "O3", "M0", "F21", "S", "V0", "F22", "F23", "A0", "A1", "M1", "V1",
+    "s0", "A2", "a", "D0", "s1", "G0:3", "s2", "wT01", "G0:2", "s3", "w2Ps", "G0:1", "H", "P", "wS",
+    "G0:0", "E", "wRp",
+)
 route_scale = 2.5
 norm_eps = 1e-06
 vmem_bytes = 67043328
@@ -777,7 +783,7 @@
     lanes = -(-2 * E // 128) * 128
     bf16, f32 = jnp.bfloat16, jnp.float32
     halves = 1 if C % 256 == 0 and C >= 1024 else 1
-    modes = "A" if C % 512 == 0 and C >= 1024 else "A"
+    modes = "A"
     P = len(modes)
     columns = Y if "B" in modes else 1
     Q = 2 + halves

time: 147 us -> 145 us (0.986)
  the two profiles are of different devices: /device:TPU:12 before, /device:TPU:1 now
where the time goes in v4:
time: 145 us; the launch traced here: 143 us
  Pallas kernels  143 us (99%)
    pallas_call x1, Pallas kernels, body(): pl.pallas_call(functools.partial(handover, dims), out_shape=[pltpu.VMEM((...  139 us
    pallas_call x1, Pallas kernels, emit(): pl.pallas_call(emit_kernel, out_shape=[jax.ShapeDtypeStruct(s, jnp.bfloat...  3.8 us

profile of v4, /device:TPU:1, one launch (start us, length us, event | category | flops | bytes accessed | tf_op | source)
XLA Modules:
  0.0 143.5 jit_solution(15392725678054392541)
XLA Ops:
  0.6 139.0 %handover.1 = (bf16[176,1024]{1,0:T(8,128)(2,1)S(1)}, bf16[2,512,1024]{2,1,0:T(8,128)(2,1)S(1)}, bf16[2,512,1024]{2,1,0:T(8,128)(2,1)S(1)}, bf16[2,512,1024]{2,1,0:T(8,128)(2,1)S(1)}, bf16[3,512,1024]{2,1,0:T(8,128)(2,1)S(1)}) custom-call(bf16[176,2048]{1,0:T(8,128)(2,1)} %tok.1, s32[8,176]{1,0:T(8,128)} %bitcast.3, f32[8,176]{1,0:T(8,128)} %bitcast.4, ...), custom_call_target="tpu_custom_call" | custom-call | tf_op jit(solution)/shard_map/handover/pallas_call | solution.py:799
  139.7 3.8 %emit.1 = (bf16[176,1024]{1,0:T(8,128)(2,1)}, bf16[2,1,512,1024]{3,2,1,0:T(8,128)(2,1)}, bf16[2,1,512,1024]{3,2,1,0:T(8,128)(2,1)}, bf16[2,1,512,1024]{3,2,1,0:T...) custom-call(bf16[176,1024]{1,0:T(8,128)(2,1)S(1)} %get-tuple-element.12.mixed, ...), custom_call_target="tpu_custom_call" | custom-call | tf_op jit(solution)/shard_map/emit/pallas_call | solution.py:753

commit v5 on v4

--- a/solution.py
+++ b/solution.py
@@ -397,7 +397,7 @@
         place = act.at[j, rows(s, NH, NH)]
         return rdma(place, place, a_send.at[j, t], a_recv.at[j, s], {"tp": t})
 
-    PB = 2 if NB % 2 == 0 else 1
+    PB = 4 if NB % 4 == 0 else 2 if NB % 2 == 0 else 1
 
     def first_matmuls(j):
         g = gr_peer(j)
@@ -737,9 +737,13 @@
 def emit_kernel(mixed, n0, n1, n2, hs, *refs):
     sem = refs[-1]
     sources = [mixed, n0, n1, n2, hs.at[0], hs.at[1], hs.at[2]]
-    copies = []
+    pairs = []
     for i, (src, dst) in enumerate(zip(sources, refs[:-1])):
-        copies.append(pltpu.make_async_copy(src, dst.at[:, 0] if 0 < i < 4 else dst, sem.at[i]))
+        if 0 < i < 4:
+            pairs += [(src.at[g], dst.at[g, 0]) for g in range(src.shape[0])]
+        else:
+            pairs.append((src, dst))
+    copies = [pltpu.make_async_copy(src, dst, sem.at[i]) for i, (src, dst) in enumerate(pairs)]
     for copy in copies:
         copy.start()
     for copy in copies:
@@ -755,7 +759,7 @@
         out_shape=[jax.ShapeDtypeStruct(s, jnp.bfloat16) for s in shapes],
         in_specs=[pl.BlockSpec(memory_space=pltpu.VMEM)] * len(results),
         out_specs=[pl.BlockSpec(memory_space=pl.ANY)] * len(shapes),
-        scratch_shapes=[pltpu.SemaphoreType.DMA((len(shapes),))],
+        scratch_shapes=[pltpu.SemaphoreType.DMA((len(shapes) + 3 * (G - 1),))],
         compiler_params=pltpu.CompilerParams(vmem_limit_bytes=vmem_bytes // 2),
         name="emit",
     )(*results)

time: 145 us -> 144 us (level)
  no operation moved by 1% of the time
where the time goes in v5:
time: 144 us; the launch traced here: 143 us
  Pallas kernels  142 us (99%)
    pallas_call x1, Pallas kernels, body(): pl.pallas_call(functools.partial(handover, dims), out_shape=[pltpu.VMEM((...  138 us
    pallas_call x1, Pallas kernels, emit(): pl.pallas_call(emit_kernel, out_shape=[jax.ShapeDtypeStruct(s, jnp.bfloat...  3.82 us

profile of v5, /device:TPU:1, one launch (start us, length us, event | category | flops | bytes accessed | tf_op | source)
XLA Modules:
  0.0 142.8 jit_solution(125291576204581807)
XLA Ops:
  0.6 138.3 %handover.1 = (bf16[176,1024]{1,0:T(8,128)(2,1)S(1)}, bf16[2,512,1024]{2,1,0:T(8,128)(2,1)S(1)}, bf16[2,512,1024]{2,1,0:T(8,128)(2,1)S(1)}, bf16[2,512,1024]{2,1,0:T(8,128)(2,1)S(1)}, bf16[3,512,1024]{2,1,0:T(8,128)(2,1)S(1)}) custom-call(bf16[176,2048]{1,0:T(8,128)(2,1)} %tok.1, s32[8,176]{1,0:T(8,128)} %bitcast.3, f32[8,176]{1,0:T(8,128)} %bitcast.4, ...), custom_call_target="tpu_custom_call" | custom-call | tf_op jit(solution)/shard_map/handover/pallas_call | solution.py:803
  139.0 3.8 %emit.1 = (bf16[176,1024]{1,0:T(8,128)(2,1)}, bf16[2,1,512,1024]{3,2,1,0:T(8,128)(2,1)}, bf16[2,1,512,1024]{3,2,1,0:T(8,128)(2,1)}, bf16[2,1,512,1024]{3,2,1,0:T...) custom-call(bf16[176,1024]{1,0:T(8,128)(2,1)S(1)} %get-tuple-element.12.mixed, ...), custom_call_target="tpu_custom_call" | custom-call | tf_op jit(solution)/shard_map/emit/pallas_call | solution.py:757
